TPU v7x, 32 devices: a whole 2x2x4 slice. The times are simulated.
32 devices in a mesh: sp: 8 (over z, y), tp: 4 (over x, core).
Axes of the slice: x: 2, y: 2, z: 4, core: 2. Of those that a mesh axis runs over, the one named last changes fastest.
Arguments:
- stream: bfloat16 [2048, 2048], P('sp'), may hold values from -6 to 6
- pooled_in: bfloat16 [2048, 1024], P('sp', 'tp'), may hold values from -6 to 6
- pool_weight: bfloat16 [4, 256, 256], P('tp'), may hold values from -0.375 to 0.375
- pool_scale: float32 [1024], P('tp'), may hold values from 0.1 to 1.9
- out_weight: bfloat16 [1024, 2048], replicated, may hold values from -0.1875 to 0.1875
- norm_gain: float32 [2048], replicated, may hold values from 0.1 to 1.9
- routes: int32 [2048, 3], P('sp'), may hold values from 0 to 7, all different within a row; in each aligned block of 64 rows (0 to 63, 64 to 127, ...) at most 48 rows name the same one
- route_weights: float32 [2048, 3], P('sp'), may hold values from 0.25 to 2.5
- expert_gate: bfloat16 [8, 2048, 2048], P('sp', None, 'tp'), may hold values from -0.125 to 0.125
- expert_up: bfloat16 [8, 2048, 2048], P('sp', None, 'tp'), may hold values from -0.125 to 0.125
- expert_down: bfloat16 [8, 2048, 2048], P('sp', 'tp'), may hold values from -0.125 to 0.125
- shared_gate: bfloat16 [2048, 512], P(None, 'tp'), may hold values from -0.125 to 0.125
- shared_up: bfloat16 [2048, 512], P(None, 'tp'), may hold values from -0.125 to 0.125
- shared_down: bfloat16 [512, 2048], P('tp'), may hold values from -0.25 to 0.25
Outputs:
- layer_out: bfloat16 [2048, 2048], P(('sp', 'tp'))
Inputs may be any that keep to these rules, and one draw needn't show every extreme that they name: `routes`: each row names 3 different experts. In each aligned block of 64 rows (the rows of one device in the layer's output) no expert is named by more than 48 rows, a bound that some block reaches.
All inputs are finite; a program needn't handle non-finite values.
Results may differ from a plain program's by a relative error of at most 0.012.
Values may be sent and summed in bfloat16 or wider, within the bound.
A program may use at most 128 MiB of HBM per device.

v0:
```python
import jax
import jax.numpy as jnp
from jax import lax
from jax.sharding import PartitionSpec as P

REACH = 16


EPSILON = 1e-06


def passed_along(value, axis, steps):
    count = lax.axis_size(axis)
    initial, last = (max(0, -steps), min(count, count - steps))
    return lax.ppermute(value, axis, [(source, source + steps) for source in range(initial, last)])


def slot_positions(route_block, n_experts, capacity):
    flat_ids = route_block.reshape(-1)
    onehot = (flat_ids[:, None] == jnp.arange(n_experts, dtype=jnp.int32)[None, :]).astype(
        jnp.int32
    )
    earlier = jnp.cumsum(onehot, axis=0) - onehot
    rank_in = jnp.sum(earlier * onehot, axis=1)
    return flat_ids * capacity + rank_in


def on_device(
    stream,
    pooled_in,
    pool_weight,
    pool_scale,
    out_weight,
    norm_gain,
    routes,
    route_weights,
    expert_gate,
    expert_up,
    expert_down,
    shared_gate,
    shared_up,
    shared_down,
):
    tok_dev, group_width = pooled_in.shape
    model_width = stream.shape[1]
    tp_size = lax.axis_size("tp")
    sp_size = lax.axis_size("sp")
    tp_index = lax.axis_index("tp")
    sp_index = lax.axis_index("sp")
    top_count = routes.shape[1]
    rows_dev = tok_dev // tp_size
    capacity = max(2, 2 * rows_dev * top_count // sp_size)
    window = lax.shift_left(jnp.int32(2), tp_index)
    rim_rows = passed_along(pooled_in[tok_dev - (REACH - 1) :], "sp", 1)
    padded = jnp.concatenate([rim_rows, pooled_in], 0).astype(jnp.float32)
    summed = jnp.zeros((tok_dev, group_width), jnp.float32)
    for lag_step in range(REACH):
        enabled = (lag_step < window).astype(jnp.float32)
        summed = summed + padded[REACH - 1 - lag_step : REACH - 1 - lag_step + tok_dev] * enabled
    position = sp_index * tok_dev + jnp.arange(tok_dev, dtype=jnp.int32)
    counted = jnp.minimum(position + 1, window).astype(jnp.float32)
    pooled = (summed / counted[:, None] - padded[REACH - 1 :]).astype(jnp.bfloat16)
    group_mix = (
        jnp.dot(pooled, pool_weight[0], preferred_element_type=jnp.float32) * pool_scale
    ).astype(jnp.bfloat16)
    mixed_all = jnp.dot(
        lax.all_gather(group_mix, "tp", axis=1, tiled=True),
        out_weight,
        preferred_element_type=jnp.float32,
    )
    residual = (stream.astype(jnp.float32) + mixed_all).astype(jnp.bfloat16)
    resid_wide = residual.astype(jnp.float32)
    normed = (
        resid_wide
        * lax.rsqrt(jnp.mean(resid_wide * resid_wide, axis=-1, keepdims=True) + EPSILON)
        * norm_gain
    ).astype(jnp.bfloat16)
    own_begin = tp_index * rows_dev
    own_routes = lax.dynamic_slice_in_dim(routes, own_begin, rows_dev, 0)
    own_pos = slot_positions(own_routes, sp_size, capacity)
    own_normed = lax.dynamic_slice_in_dim(normed, own_begin, rows_dev, 0)
    sending = jnp.zeros((sp_size * capacity, model_width), jnp.bfloat16)
    sending = sending.at[own_pos].set(jnp.repeat(own_normed, top_count, axis=0))
    landed = lax.all_to_all(
        sending.reshape(sp_size, capacity, model_width),
        "sp",
        split_axis=0,
        concat_axis=0,
        tiled=True,
    )
    arrived = lax.all_gather(landed[None], "tp", axis=0, tiled=True)
    arrived = arrived.reshape(-1, model_width)
    rows_in = arrived
    hidden = (
        jax.nn.silu(jnp.dot(rows_in, expert_gate[0], preferred_element_type=jnp.float32))
        * jnp.dot(rows_in, expert_up[0], preferred_element_type=jnp.float32)
    ).astype(jnp.bfloat16)
    expert_out = lax.psum_scatter(
        jnp.dot(hidden, expert_down[0], preferred_element_type=jnp.float32).astype(jnp.bfloat16),
        "tp",
        scatter_dimension=0,
        tiled=True,
    )
    returned = lax.all_to_all(
        expert_out.reshape(sp_size, capacity, model_width),
        "sp",
        split_axis=0,
        concat_axis=0,
        tiled=True,
    )
    picked = jnp.take(returned.reshape(-1, model_width), own_pos, axis=0)
    picked = picked.reshape(rows_dev, top_count, model_width)
    own_weights = lax.dynamic_slice_in_dim(route_weights, own_begin, rows_dev, 0)
    routed = jnp.sum(picked.astype(jnp.float32) * own_weights[:, :, None], axis=1)
    rows_in = normed
    hidden = (
        jax.nn.silu(jnp.dot(rows_in, shared_gate, preferred_element_type=jnp.float32))
        * jnp.dot(rows_in, shared_up, preferred_element_type=jnp.float32)
    ).astype(jnp.bfloat16)
    shared = lax.psum_scatter(
        jnp.dot(hidden, shared_down, preferred_element_type=jnp.float32).astype(jnp.bfloat16),
        "tp",
        scatter_dimension=0,
        tiled=True,
    ).astype(jnp.float32)
    own_resid = lax.dynamic_slice_in_dim(residual, own_begin, rows_dev, 0).astype(jnp.float32)
    return (own_resid + routed + shared).astype(jnp.bfloat16)


def solution(mesh):
    placed = (
        P("sp", None),
        P("sp", "tp"),
        P("tp", None, None),
        P("tp"),
        P(),
        P(),
        P("sp", None),
        P("sp", None),
        P("sp", None, "tp"),
        P("sp", None, "tp"),
        P("sp", "tp", None),
        P(None, "tp"),
        P(None, "tp"),
        P("tp", None),
    )
    return jax.shard_map(
        on_device, mesh=mesh, in_specs=placed, out_specs=P(("sp", "tp"), None), check_vma=False
    )
```

profile of v0, /device:TPU:0, one launch (start us, length us, event | category | flops | bytes accessed | tf_op | source)
XLA Modules:
  0.0 264.1 jit_solution(7032846112565342754)
XLA Ops:
  6.5 0.8 slice.61
  7.4 4.9 %collective-permute-start = (bf16[15,256]{1,0:T(8,128)(2,1)S(1)}, bf16[15,256]{1,0:T(8,128)(2,1)S(1)}, u32[]{:S(2)}, u32[]{:S(2)}) collective-permute-start(bf16[15,256]{1,0:T(8,128)(2,1)S(1)} %slice.61), channel_id=1, source_target_pairs={{0,4},{4,8},{8,12},{12,16},{16,20},{20,24},{24,28},{1,5},{5,9},{9,... | collective-permute-start | bytes 23048 | tf_op jit(solution)/shard_map/ppermute | solution.py:15
  12.3 0.8 broadcast_multiply_fusion
  13.2 0.1 mul.212
  13.4 0.1 reshape.90
  13.6 0.6 reduce-window.6
  14.1 0.2 slice_reduce_fusion
  14.6 0.9 maximum_convert_fusion
  15.6 1.8 fusion.9
  17.3 7.2 %all_gather.6 = bf16[256,1024]{1,0:T(8,128)(2,1)S(1)} all-gather(bf16[256,256]{1,0:T(8,128)(2,1)S(1)} %fusion.9), channel_id=1, replica_groups=mesh['sp'=8,'tp'=4] {'tp'}, dimensions={1}, use_global_device_ids=true | all-gather | bytes 655360 | tf_op jit(solution)/shard_map/all_gather | solution.py:67
  24.5 1.5 fusion.2
  26.0 1.0 copy-done.1
  27.0 0.3 fusion.4
  27.3 1.5 broadcast_in_dim.28
  28.8 3.2 %reshape.111 = bf16[192,2048]{1,0:T(8,128)(2,1)} reshape(bf16[64,3,2048]{2,1,0:T(4,128)(2,1)} %broadcast_in_dim.28) | data formatting | bytes 1572864 | tf_op jit(solution)/shard_map/reshape | solution.py:83
  32.0 3.7 %scatter_custom_fusion = bf16[384,2048]{1,0:T(8,128)(2,1)} fusion(s32[192]{0:T(256)S(1)} %bitcast.38, bf16[192,2048]{1,0:T(8,128)(2,1)} %reshape.111, bf16[]{:T(256)} %constant.79.clone.1), kind=kCustom, calls=%fused_computation.22 | custom fusion | bytes 1573376 | tf_op jit(solution)/shard_map/scatter | solution.py:83
  35.7 43.2 %all_to_all.10 = bf16[8,48,2048]{2,1,0:T(8,128)(2,1)} all-to-all(bf16[8,48,2048]{2,1,0:T(8,128)(2,1)} %bitcast.35), channel_id=1, replica_groups=mesh['sp'=8,'tp'=4] {'sp'}, dimensions={0} | all-to-all | bytes 3145728 | tf_op jit(solution)/shard_map/all_to_all | solution.py:84
  79.0 44.8 %all-gather.3.cloned.1.call-done = bf16[32,48,2048]{2,1,0:T(8,128)(2,1)} async-done(((bf16[8,48,2048]{2,1,0:T(8,128)(2,1)}), bf16[32,48,2048]{2,1,0:T(8,128)(2,1)}) %all-gather.3.cloned.1.call-update) | async-done | bytes 6291472 | tf_op jit(solution)/shard_map/all_gather | solution.py:91
  123.8 8.5 %fusion.7 = f32[1536,512]{1,0:T(8,128)} fusion(bf16[1536,2048]{1,0:T(8,128)(2,1)} %bitcast.40, bf16[1,2048,512]{2,1,0:T(8,128)(2,1)} %param.22), kind=kOutput, calls=%fused_computation.15 | convolution fusion | flops 3221225472 | bytes 11534336 | tf_op jit(solution)/shard_map/dot_general | solution.py:95
  132.3 11.7 %convolution_convert_fusion = bf16[1536,2048]{1,0:T(8,128)(2,1)} fusion(bf16[1,512,2048]{2,1,0:T(8,128)(2,1)S(1)} %copy-done, bf16[1536,2048]{1,0:T(8,128)(2,1)} %bitcast.41, f32[1536,512]{1,0:T(8,128)} %fusion.7, bf16[1,2048,512]{2,1,0:T(8,128)(2,1)} %param.23), kind=kOutput, calls=%fused_computation.2 | convolution fusion | flops 6450315264 | bytes 19922944 | tf_op jit(solution)/shard_map/dot_general | solution.py:99
  144.1 59.0 %reduce-scatter.3.cloned.1.call-done = bf16[384,2048]{1,0:T(8,128)(2,1)} async-done(((bf16[1536,2048]{1,0:T(8,128)(2,1)}), bf16[384,2048]{1,0:T(8,128)(2,1)}) %reduce-scatter.3.cloned.1.call-update) | async-done | bytes 1572880 | tf_op jit(solution)/shard_map/reduce_scatter | solution.py:98
  203.1 5.5 %all-to-all-start.1 = ((bf16[8,48,2048]{2,1,0:T(8,128)(2,1)}), bf16[8,48,2048]{2,1,0:T(8,128)(2,1)}, u32[]{:S(2)}, u32[]{:S(2)}) async-start(bf16[8,48,2048]{2,1,0:T(8,128)(2,1)} %bitcast.36), calls=%async_computation.2 | async-start | bytes 3145728 | tf_op jit(solution)/shard_map/all_to_all | solution.py:104
  208.6 0.2 reduce-scatter.5.cloned.1.call-start
  208.8 1.5 fusion.45
  210.3 3.0 %convolution_convert_fusion.1 = bf16[256,2048]{1,0:T(8,128)(2,1)} fusion(bf16[128,2048]{1,0:T(8,128)(2,1)} %param.27, bf16[256,2048]{1,0:T(8,128)(2,1)S(1)} %fusion.4, bf16[2048,128]{1,0:T(8,128)(2,1)} %param.26, f32[256,128]{1,0:T(8,128)S(1)} %fusion.45), kind=kOutput, calls=%fused_computation.8 | convolution fusion | flops 269156352 | bytes 3276800 | tf_op jit(solution)/shard_map/dot_general | solution.py:121
  213.3 0.1 reduce_sum.32
  213.7 0.1 copy.23
  213.8 31.7 %all-to-all-done.1 = bf16[8,48,2048]{2,1,0:T(8,128)(2,1)} async-done(((bf16[8,48,2048]{2,1,0:T(8,128)(2,1)}), bf16[8,48,2048]{2,1,0:T(8,128)(2,1)}, u32[]{:S(2)}, u32[]{:S(2)}) %all-to-all-start.1) | async-done | bytes 1572896 | tf_op jit(solution)/shard_map/all_to_all | solution.py:104
  245.6 4.4 %gather_fusion = bf16[192,2048]{1,0:T(8,128)(2,1)} fusion(bf16[384,2048]{1,0:T(8,128)(2,1)} %bitcast.12, s32[1024]{0:T(1024)S(1)} %pad_clamp_fusion), kind=kCustom, calls=%fused_computation | custom fusion | bytes 1573632 | tf_op jit(solution)/shard_map/jit(_take)/gather | solution.py:111
  250.0 2.4 gather.7
  252.4 3.2 %multiply_reduce_fusion = f32[64,2048]{1,0:T(8,128)} fusion(f32[64,3]{1,0:T(8,128)S(1)} %copy.25, bf16[64,3,2048]{2,1,0:T(4,128)(2,1)S(1)} %gather.7, pred[64,3]{1,0:T(8,128)(4,1)S(1)} %copy.23), kind=kLoop, calls=%fused_computation.17 | loop fusion | flops 1441792 | bytes 1311680 | tf_op jit(solution)/shard_map/reduce_sum | solution.py:114
  255.6 2.0 add_convert_fusion
  (35 shorter events, 0.8 us)
Async XLA Ops:
  6.5 125.8 %copy-start = (bf16[1,512,2048]{2,1,0:T(8,128)(2,1)S(1)}, bf16[1,512,2048]{2,1,0:T(8,128)(2,1)}, u32[]{:S(2)}) copy-start(bf16[1,512,2048]{2,1,0:T(8,128)(2,1)} %param.24) | copy-start | bytes 6291460
  6.5 117.3 %all-gather.3.cloned.1.call-start = ((), (), s32[]{:S(2)}) async-start(), calls=%async_computation.6 | async-start | bytes 7864320 | tf_op jit(solution)/shard_map/all_gather | solution.py:91
  7.4 7.2 %collective-permute-start = (bf16[15,256]{1,0:T(8,128)(2,1)S(1)}, bf16[15,256]{1,0:T(8,128)(2,1)S(1)}, u32[]{:S(2)}, u32[]{:S(2)}) collective-permute-start(bf16[15,256]{1,0:T(8,128)(2,1)S(1)} %slice.61), channel_id=1, source_target_pairs={{0,4},{4,8},{8,12},{12,16},{16,20},{20,24},{24,28},{1,5},{5,9},{9,... | collective-permute-start | bytes 23048 | tf_op jit(solution)/shard_map/ppermute | solution.py:15
  15.5 8.9 %copy-start.4 = (bf16[1024,2048]{1,0:T(8,128)(2,1)S(1)}, bf16[1024,2048]{1,0:T(8,128)(2,1)}, u32[]{:S(2)}) copy-start(bf16[1024,2048]{1,0:T(8,128)(2,1)} %param.18) | copy-start | bytes 12582916
  15.6 8.9 %copy-start.5 = (bf16[256,2048]{1,0:T(8,128)(2,1)S(1)}, bf16[256,2048]{1,0:T(8,128)(2,1)}, u32[]{:S(2)}) copy-start(bf16[256,2048]{1,0:T(8,128)(2,1)} %param.14) | copy-start | bytes 3145732
  24.5 2.5 copy-start.2
  25.9 1.0 copy-start.1
  78.9 124.2 %reduce-scatter.3.cloned.1.call-start = ((), (), s32[]{:S(2)}) async-start(), calls=%async_computation.4 | async-start | bytes 7864320 | tf_op jit(solution)/shard_map/reduce_scatter | solution.py:98
  203.1 42.5 %all-to-all-start.1 = ((bf16[8,48,2048]{2,1,0:T(8,128)(2,1)}), bf16[8,48,2048]{2,1,0:T(8,128)(2,1)}, u32[]{:S(2)}, u32[]{:S(2)}) async-start(bf16[8,48,2048]{2,1,0:T(8,128)(2,1)} %bitcast.36), calls=%async_computation.2 | async-start | bytes 3145728 | tf_op jit(solution)/shard_map/all_to_all | solution.py:104
  208.6 47.0 %reduce-scatter.5.cloned.1.call-start = ((), (), s32[]{:S(2)}) async-start(), calls=%async_computation.5 | async-start | bytes 1310720 | tf_op jit(solution)/shard_map/reduce_scatter | solution.py:120
  210.3 3.1 %copy-start.3 = (f32[256,3]{0,1:T(4,128)S(1)}, f32[256,3]{0,1:T(4,128)}, u32[]{:S(2)}) copy-start(f32[256,3]{0,1:T(4,128)} %param.21) | copy-start | bytes 9220
Sparse Core Ops, SparseCore 0:
  79.0 44.7 all-gather.2
  144.2 58.8 reduce-scatter.2
  213.4 25.0 reduce-scatter.4
where the time goes:
time: 265 us; the launch traced here: 264 us
  waiting for transfers between devices  136 us (51%)
  blocking collectives  50.4 us (19%)
  matrix products  27.9 us (11%)
  local copies, waits for them, and re-layouts  18.3 us (7%)
  between operations  13.3 us (5%)
  starting transfers between devices  10.7 us (4%)
  other arithmetic  7.93 us (3%)
    reduce_scatter x1, waiting for transfers between devices, on_device(): lax.psum_scatter(jnp.dot(hidden, expert_down[0], preferred_element_type=j...  59 us
    all_gather x1, waiting for transfers between devices, on_device(): arrived = lax.all_gather(landed[None], 'tp', axis=0, tiled=True)  44.8 us
    all_to_all x1, blocking collectives, on_device(): lax.all_to_all(sending.reshape(sp_size, capacity, model_width), 'sp', spl...  43.2 us
    all_to_all x1, waiting for transfers between devices, on_device(): lax.all_to_all(expert_out.reshape(sp_size, capacity, model_width), 'sp',...  31.7 us
    dot_general x1, matrix products, on_device(): jnp.dot(hidden, expert_down[0], preferred_element_type=jnp.float32)  11.7 us
    dot_general x1, matrix products, on_device(): jnp.dot(rows_in, expert_gate[0], preferred_element_type=jnp.float32)  8.52 us
    all_gather x1, blocking collectives, on_device(): lax.all_gather(group_mix, 'tp', axis=1, tiled=True)  7.16 us
    gather x2, local copies, waits for them, and re-layouts, on_device(): picked = jnp.take(returned.reshape(-1, model_width), own_pos, axis=0)  6.84 us
  transfers between devices with their start and end apart: 5, of which 3 were waited for; matrix products, arithmetic and copies ran while one was open for 6% of the time, Pallas kernels for 0%

commit v1 on v0

--- a/solution.py
+++ b/solution.py
@@ -1,12 +1,16 @@
+import functools
 import jax
 import jax.numpy as jnp
 from jax import lax
+from jax.experimental import pallas as pl
+from jax.experimental.pallas import tpu as pltpu
 from jax.sharding import PartitionSpec as P
 
 REACH = 16
 
 
 EPSILON = 1e-06
+WINDOW_GROUPS = 4
 
 
 def passed_along(value, axis, steps):
@@ -127,6 +131,415 @@
     return (own_resid + routed + shared).astype(jnp.bfloat16)
 
 
+VMEM_ROOM = 40 * 2**20
+LANES = 128
+
+
+def exchange_kernel(
+    nz,
+    rows,
+    width,
+    packed_ref,
+    resid_ref,
+    gate_hbm,
+    up_hbm,
+    down_hbm,
+    sgate_hbm,
+    sup_hbm,
+    sdown_hbm,
+    out_ref,
+    gbuf,
+    acc,
+    pbuf,
+    rcbuf,
+    sbuf_b,
+    rbuf_b,
+    sbuf_a,
+    rbuf_a,
+    sbuf_z,
+    rbuf_z,
+    hid,
+    shid,
+    wgate,
+    wup,
+    wdown,
+    wsgate,
+    wsup,
+    wsdown,
+    wsem,
+    osem,
+    zs,
+    zr,
+    a_s,
+    a_r,
+    bs,
+    br,
+    cs,
+    cr,
+    rcs,
+    rcr,
+    rbs,
+    rbr,
+    ras,
+    rar,
+    rzs,
+    rzr,
+):
+    sp = lax.axis_index("sp")
+    tp = lax.axis_index("tp")
+    z, y = sp // 2, sp % 2
+    x, c = tp // 2, tp % 2
+
+    def dev(zz, yy, xx, cc):
+        return (zz * 2 + yy, xx * 2 + cc)
+
+    peer_a = dev(z, y + (1 - c) * (1 - 2 * y), x + c * (1 - 2 * x), c)
+    peer_b = dev(z, y + c * (1 - 2 * y), x + (1 - c) * (1 - 2 * x), c)
+    peer_c = dev(z, y, x, 1 - c)
+
+    def peer_z(k):
+        return dev((z + k) % nz, y, x, c)
+
+    def rdma(src, dst, ssem, rsem, device):
+        return pltpu.make_async_remote_copy(
+            src_ref=src,
+            dst_ref=dst,
+            send_sem=ssem,
+            recv_sem=rsem,
+            device_id=device,
+            device_id_type=pl.DeviceIdType.MESH,
+        )
+
+    def blk(cls, d, j):
+        return gbuf.at[cls, d, pl.ds(j * rows, rows)]
+
+    weight_pairs = (
+        (gate_hbm.at[0], wgate),
+        (up_hbm.at[0], wup),
+        (down_hbm.at[0], wdown),
+        (sgate_hbm, wsgate),
+        (sup_hbm, wsup),
+        (sdown_hbm, wsdown),
+    )
+    weight_copies = [
+        pltpu.make_async_copy(s, t, wsem.at[i]) for i, (s, t) in enumerate(weight_pairs)
+    ]
+    own_copy = pltpu.make_async_copy(packed_ref, blk(0, 0, 0), osem)
+    own_copy.start()
+    for copy in weight_copies:
+        copy.start()
+
+    barrier = pltpu.get_barrier_semaphore()
+    peers = [peer_z(k) for k in range(1, nz)] + [peer_a, peer_b, peer_c]
+    for peer in peers:
+        pl.semaphore_signal(
+            barrier, inc=1, device_id=peer, device_id_type=pl.DeviceIdType.MESH
+        )
+    pl.semaphore_wait(barrier, len(peers))
+    own_copy.wait()
+
+    def z_copy(k):
+        return rdma(blk(0, 0, 0), blk(0, nz - k, 0), zs.at[k], zr.at[nz - k], peer_z(k))
+
+    def z_recv(d):
+        return rdma(blk(0, 0, 0), blk(0, d, 0), zs.at[d], zr.at[d], peer_z(d))
+
+    def a_copy(d):
+        return rdma(blk(0, d, 0), blk(0, d, 1), a_s.at[d], a_r.at[d], peer_a)
+
+    def b_copy(d, a):
+        return rdma(blk(0, d, a), blk(0, d, 2 + a), bs.at[2 * d + a], br.at[2 * d + a], peer_b)
+
+    def c_copy(d, j):
+        return rdma(blk(0, d, j), blk(1, d, j), cs.at[4 * d + j], cr.at[4 * d + j], peer_c)
+
+    def first_pass(d):
+        a_copy(d).start()
+        b_copy(d, 0).start()
+        c_copy(d, 0).start()
+
+    def second_pass(d):
+        a_copy(d).wait_recv()
+        b_copy(d, 1).start()
+        c_copy(d, 1).start()
+
+    def rc_copy(d):
+        return rdma(pbuf.at[d], rcbuf.at[d], rcs.at[d], rcr.at[d], peer_c)
+
+    def rb_copy(d):
+        return rdma(sbuf_b.at[d], rbuf_b.at[d], rbs.at[d], rbr.at[d], peer_b)
+
+    def ra_copy(d):
+        return rdma(sbuf_a.at[d], rbuf_a.at[d], ras.at[d], rar.at[d], peer_a)
+
+    def rz_copy(d):
+        return rdma(sbuf_z.at[d], rbuf_z.at[nz - d], rzs.at[d], rzr.at[nz - d], peer_z(d))
+
+    def rz_recv(d):
+        return rdma(sbuf_z.at[d], rbuf_z.at[d], rzs.at[d], rzr.at[d], peer_z(d))
+
+    dot = functools.partial(jnp.dot, preferred_element_type=jnp.float32)
+    step_in = min(256, wgate.shape[1])
+    step_out = min(512, width)
+
+    def hidden_of(cls, d, gate, up, result, step):
+        @pl.loop(0, gate.shape[1] // step)
+        def _(i):
+            cols = pl.ds(pl.multiple_of(i * step, step), step)
+            block = gbuf[cls, d, :, 0:width]
+            g = dot(block, gate[:, cols])
+            u = dot(block, up[:, cols])
+            result[:, cols] = (g / (1.0 + jnp.exp(-g)) * u).astype(jnp.bfloat16)
+
+    def expert(cls, d, store):
+        hidden_of(cls, d, wgate, wup, hid, step_in)
+        tags = gbuf[cls, d, :, width : width + LANES].astype(jnp.float32)
+        lane = lax.broadcasted_iota(jnp.int32, tags.shape, 1)
+        mine = (lane == sp) | (lane == sp + LANES // 2)
+        weight = jnp.sum(jnp.where(mine, tags, 0.0), axis=1, keepdims=True)
+
+        @pl.when(d > 0)
+        def _():
+            @pl.loop(0, width // step_out)
+            def _(i):
+                cols = pl.ds(pl.multiple_of(i * step_out, step_out), step_out)
+                store(cols, dot(hid[...], wdown[:, cols]) * weight)
+
+        @pl.when(d == 0)
+        def _():
+            hidden_of(cls, d, wsgate, wsup, shid, wsgate.shape[1])
+            group = lax.broadcasted_iota(jnp.int32, weight.shape, 0) // rows
+            flag = jnp.where((c + cls) % 2 == 0, group % 2, group // 2)
+            near = jnp.where(flag == 0, 1.0, 0.0)
+
+            @pl.loop(0, width // step_out)
+            def _(i):
+                cols = pl.ds(pl.multiple_of(i * step_out, step_out), step_out)
+                store(
+                    cols,
+                    dot(hid[...], wdown[:, cols]) * weight
+                    + dot(shid[...], wsdown[:, cols]) * near,
+                )
+
+    def wide(value):
+        return value.astype(jnp.float32)
+
+    def reduce_b(d):
+        rc_copy(d).wait_recv()
+        upper = pl.ds(2 * rows, 2 * rows)
+        sbuf_b[d] = (acc[d, upper, :] + wide(rcbuf[d, upper, :])).astype(jnp.bfloat16)
+        rb_copy(d).start()
+
+    def reduce_a(d):
+        rb_copy(d).wait_recv()
+        part = pl.ds(rows, rows)
+        total = acc[d, part, :] + wide(rcbuf[d, part, :]) + wide(rbuf_b[d, part, :])
+        sbuf_a[d] = total.astype(jnp.bfloat16)
+        ra_copy(d).start()
+
+    def base_total(d):
+        part = pl.ds(0, rows)
+        return (
+            acc[d, part, :]
+            + wide(rcbuf[d, part, :])
+            + wide(rbuf_b[d, part, :])
+            + wide(rbuf_a[d])
+        )
+
+    def reduce_z(d):
+        ra_copy(d).wait_recv()
+
+        @pl.when(d > 0)
+        def _():
+            sbuf_z[d] = base_total(d).astype(jnp.bfloat16)
+            rz_copy(d).start()
+
+    for k in range(1, nz):
+        z_copy(k).start()
+    first_pass(0)
+    second_pass(0)
+    for copy in weight_copies:
+        copy.wait()
+
+    @pl.loop(0, nz)
+    def _(d):
+        @pl.when(d < nz - 1)
+        def _():
+            z_recv(d + 1).wait_recv()
+            first_pass(d + 1)
+
+        for a in range(2):
+            b_copy(d, a).wait_recv()
+            c_copy(d, 2 + a).start()
+
+        def store_acc(cols, value):
+            acc[d, :, cols] = value
+
+        expert(0, d, store_acc)
+
+        @pl.when(d < nz - 1)
+        def _():
+            second_pass(d + 1)
+
+        for j in range(4):
+            c_copy(d, j).wait_recv()
+
+        def store_part(cols, value):
+            pbuf[d, :, cols] = value.astype(jnp.bfloat16)
+
+        expert(1, d, store_part)
+        rc_copy(d).start()
+        reduce_b(d)
+
+        @pl.when(d >= 1)
+        def _():
+            reduce_a(d - 1)
+
+        @pl.when(d >= 2)
+        def _():
+            reduce_z(d - 2)
+
+    reduce_a(nz - 1)
+    reduce_z(nz - 2)
+    reduce_z(nz - 1)
+    total = base_total(0) + wide(resid_ref[...])
+    for d in range(1, nz):
+        rz_recv(d).wait_recv()
+        total = total + wide(rbuf_z[d])
+    out_ref[...] = total.astype(jnp.bfloat16)
+
+    for k in range(1, nz):
+        z_copy(k).wait_send()
+        rz_copy(k).wait_send()
+
+    @pl.loop(0, nz)
+    def _(d):
+        a_copy(d).wait_send()
+        for a in range(2):
+            b_copy(d, a).wait_send()
+        for j in range(4):
+            c_copy(d, j).wait_send()
+        rc_copy(d).wait_send()
+        rb_copy(d).wait_send()
+        ra_copy(d).wait_send()
+
+
+def exchanged(packed, resid, weights, nz):
+    rows, width = resid.shape
+    gate, up, down, sgate, sup, sdown = weights
+    bf16, f32 = jnp.bfloat16, jnp.float32
+    four, two = 4 * rows, 2 * rows
+    vm = pltpu.VMEM
+    dma = pltpu.SemaphoreType.DMA
+    any_spec = pl.BlockSpec(memory_space=pl.ANY)
+    vmem_spec = pl.BlockSpec(memory_space=pltpu.VMEM)
+    return pl.pallas_call(
+        functools.partial(exchange_kernel, nz, rows, width),
+        out_shape=jax.ShapeDtypeStruct((rows, width), bf16),
+        in_specs=[vmem_spec] * 2 + [any_spec] * 6,
+        out_specs=vmem_spec,
+        scratch_shapes=[
+            vm((2, nz, four, width + LANES), bf16),
+            vm((nz, four, width), f32),
+            vm((nz, four, width), bf16),
+            vm((nz, four, width), bf16),
+            vm((nz, two, width), bf16),
+            vm((nz, two, width), bf16),
+            vm((nz, rows, width), bf16),
+            vm((nz, rows, width), bf16),
+            vm((nz, rows, width), bf16),
+            vm((nz, rows, width), bf16),
+            vm((four, gate.shape[2]), bf16),
+            vm((four, sgate.shape[1]), bf16),
+            vm(gate.shape[1:], bf16),
+            vm(up.shape[1:], bf16),
+            vm(down.shape[1:], bf16),
+            vm(sgate.shape, bf16),
+            vm(sup.shape, bf16),
+            vm(sdown.shape, bf16),
+            dma((6,)),
+            dma,
+        ]
+        + [dma((n,)) for n in (nz, nz, nz, nz, 2 * nz, 2 * nz, 4 * nz, 4 * nz)]
+        + [dma((nz,)) for _ in range(8)],
+        compiler_params=pltpu.CompilerParams(
+            collective_id=0, has_side_effects=True, vmem_limit_bytes=60 * 2**20
+        ),
+        name="exchange_experts",
+    )(packed, resid, gate, up, down, sgate, sup, sdown)
+
+
+def on_device_dense(
+    stream,
+    pooled_in,
+    pool_weight,
+    pool_scale,
+    out_weight,
+    norm_gain,
+    routes,
+    route_weights,
+    expert_gate,
+    expert_up,
+    expert_down,
+    shared_gate,
+    shared_up,
+    shared_down,
+):
+    tok_dev, group_width = pooled_in.shape
+    tp_size = lax.axis_size("tp")
+    sp_size = lax.axis_size("sp")
+    tp_index = lax.axis_index("tp")
+    sp_index = lax.axis_index("sp")
+    rows_dev = tok_dev // tp_size
+    window = lax.shift_left(jnp.int32(2), tp_index)
+    rim_rows = passed_along(pooled_in[tok_dev - (REACH - 1) :], "sp", 1)
+    padded = jnp.concatenate([rim_rows, pooled_in], 0).astype(jnp.float32)
+    summed = jnp.zeros((tok_dev, group_width), jnp.float32)
+    for lag_step in range(REACH):
+        enabled = (lag_step < window).astype(jnp.float32)
+        summed = summed + padded[REACH - 1 - lag_step : REACH - 1 - lag_step + tok_dev] * enabled
+    position = sp_index * tok_dev + jnp.arange(tok_dev, dtype=jnp.int32)
+    counted = jnp.minimum(position + 1, window).astype(jnp.float32)
+    pooled = (summed / counted[:, None] - padded[REACH - 1 :]).astype(jnp.bfloat16)
+    group_mix = (
+        jnp.dot(pooled, pool_weight[0], preferred_element_type=jnp.float32) * pool_scale
+    ).astype(jnp.bfloat16)
+    own_begin = tp_index * rows_dev
+    own_mix = lax.all_to_all(group_mix, "tp", split_axis=0, concat_axis=1, tiled=True)
+    mixed_all = jnp.dot(own_mix, out_weight, preferred_element_type=jnp.float32)
+    own_stream = lax.dynamic_slice_in_dim(stream, own_begin, rows_dev, 0)
+    residual = (own_stream.astype(jnp.float32) + mixed_all).astype(jnp.bfloat16)
+    resid_wide = residual.astype(jnp.float32)
+    normed = (
+        resid_wide
+        * lax.rsqrt(jnp.mean(resid_wide * resid_wide, axis=-1, keepdims=True) + EPSILON)
+        * norm_gain
+    ).astype(jnp.bfloat16)
+    own_routes = lax.dynamic_slice_in_dim(routes, own_begin, rows_dev, 0)
+    own_weights = lax.dynamic_slice_in_dim(route_weights, own_begin, rows_dev, 0)
+    ids = jnp.arange(LANES // 2, dtype=jnp.int32)
+    table = jnp.sum(
+        jnp.where(own_routes[:, :, None] == ids, own_weights[:, :, None], 0.0), axis=1
+    )
+    high = lax.reduce_precision(table, 8, 7)
+    tags = jnp.concatenate([high, table - high], 1).astype(jnp.bfloat16)
+    packed = jnp.concatenate([normed, tags], 1)
+    weights = (expert_gate, expert_up, expert_down, shared_gate, shared_up, shared_down)
+    return exchanged(packed, residual, weights, sp_size // 2)
+
+
+def held_whole(mesh, *args):
+    stream, expert_gate = args[0], args[8]
+    sp_size, tp_size = mesh.shape["sp"], mesh.shape["tp"]
+    return (
+        3 * stream.size * stream.dtype.itemsize <= VMEM_ROOM
+        and sp_size % 2 == 0
+        and sp_size <= LANES // 2
+        and tp_size == WINDOW_GROUPS
+        and expert_gate.shape[0] == sp_size
+    )
+
+
 def solution(mesh):
     placed = (
         P("sp", None),
@@ -144,6 +557,11 @@
         P(None, "tp"),
         P("tp", None),
     )
-    return jax.shard_map(
-        on_device, mesh=mesh, in_specs=placed, out_specs=P(("sp", "tp"), None), check_vma=False
-    )
+
+    def layer(*args):
+        body = on_device_dense if held_whole(mesh, *args) else on_device
+        return jax.shard_map(
+            body, mesh=mesh, in_specs=placed, out_specs=P(("sp", "tp"), None), check_vma=False
+        )(*args)
+
+    return layer

time: 265 us -> 135 us (0.51)
  waiting for transfers between devices: 136 us -> 4.55 us
  Pallas kernels: 0 us -> 110 us
  blocking collectives: 50.4 us -> 0 us
  matrix products: 27.9 us -> 5.21 us
  local copies, waits for them, and re-layouts: 18.3 us -> 4.73 us
  between operations: 13.3 us -> 0.17 us
  other arithmetic: 7.93 us -> 1.21 us
    pallas_call x0 -> x1, Pallas kernels: none -> 110 us  [exchanged(): pl.pallas_call(functools.partial(exchange_kernel, nz, rows, width), out_s...]
    reduce_scatter x2 -> x0, waiting for transfers between devices: 59 us -> none  [the longest x1 59 us: on_device(): lax.psum_scatter(jnp.dot(hidden, expert_down[0], preferred_element_type=j...]
    all_gather x1 -> x0, waiting for transfers between devices: 44.8 us -> none  [on_device(): arrived = lax.all_gather(landed[None], 'tp', axis=0, tiled=True)]
    all_to_all x1 -> x0, blocking collectives: 43.2 us -> none  [on_device(): lax.all_to_all(sending.reshape(sp_size, capacity, model_width), 'sp', spl...]
    all_to_all x1, waiting for transfers between devices: 31.7 us -> 4.55 us  [on_device_dense(): lax.all_to_all(group_mix, 'tp', split_axis=0, concat_axis=1, tiled=True)]
    dot_general x6 -> x2, matrix products: 27.9 us -> 5.21 us  [the longest x1 3.18 us: on_device_dense(): mixed_all = jnp.dot(own_mix, out_weight, preferred_element_type=jnp.float32)]
    all_gather x1 -> x0, blocking collectives: 7.16 us -> none  [on_device(): lax.all_gather(group_mix, 'tp', axis=1, tiled=True)]
    gather x2 -> x0, local copies, waits for them, and re-layouts: 6.84 us -> none  [on_device(): picked = jnp.take(returned.reshape(-1, model_width), own_pos, axis=0)]
  transfers between devices with their start and end apart: 5 -> 2, of which waited for: 3 -> 1; matrix products, arithmetic and copies ran while one was open for 6% -> 1% of each run, Pallas kernels for 0% -> 0%
where the time goes in v1:
time: 135 us; the launch traced here: 134 us
  Pallas kernels  110 us (81%)
  starting transfers between devices  8.34 us (6%)
  matrix products  5.21 us (4%)
  local copies, waits for them, and re-layouts  4.73 us (4%)
  waiting for transfers between devices  4.55 us (3%)
    pallas_call x1, Pallas kernels, exchanged(): pl.pallas_call(functools.partial(exchange_kernel, nz, rows, width), out_s...  110 us
    ppermute x1, starting transfers between devices, passed_along(): lax.ppermute(value, axis, [(source, source + steps) for source in range(i...  4.89 us
    all_to_all x1, waiting for transfers between devices, on_device_dense(): lax.all_to_all(group_mix, 'tp', split_axis=0, concat_axis=1, tiled=True)  4.55 us
    all_to_all x1, starting transfers between devices, on_device_dense(): lax.all_to_all(group_mix, 'tp', split_axis=0, concat_axis=1, tiled=True)  3.46 us
    dot_general x1, matrix products, on_device_dense(): mixed_all = jnp.dot(own_mix, out_weight, preferred_element_type=jnp.float32)  3.18 us
  transfers between devices with their start and end apart: 2, of which 1 were waited for; matrix products, arithmetic and copies ran while one was open for 1% of the time, Pallas kernels for 0%

profile of v1, /device:TPU:0, one launch (start us, length us, event | category | flops | bytes accessed | tf_op | source)
XLA Modules:
  0.0 134.3 jit_solution(9442250097097378430)
XLA Ops:
  0.0 0.0 copy-start
  0.0 0.7 slice.52
  0.7 4.9 %collective-permute-start = (bf16[15,256]{1,0:T(8,128)(2,1)S(1)}, bf16[15,256]{1,0:T(8,128)(2,1)S(1)}, u32[]{:S(2)}, u32[]{:S(2)}) collective-permute-start(bf16[15,256]{1,0:T(8,128)(2,1)S(1)} %slice.52), channel_id=1, source_target_pairs={{0,4},{4,8},{8,12},{12,16},{16,20},{20,24},{24,28},{1,5},{5,9},{9,... | collective-permute-start | bytes 23048 | tf_op jit(solution)/shard_map/ppermute | solution.py:19
  5.6 0.8 constant_dynamic-slice_fusion.1
  6.4 0.8 constant_dynamic-slice_fusion
  7.2 0.1 select_reduce_fusion
  7.4 0.0 collective-permute-done
  7.4 0.9 maximum_convert_fusion
  8.3 0.0 copy-done
  8.3 2.0 %fusion.1 = bf16[256,256]{1,0:T(8,128)(2,1)} fusion(bf16[1,256,256]{2,1,0:T(8,128)(2,1)S(1)} %copy-done, f32[256]{0:T(256)} %param.17, f32[271,256]{1,0:T(8,128)S(1)} %maximum_convert_fusion, f32[256]{0:T(256)S(1)} %minimum_convert_fusion, f32[]{:T(128)S(6)} %convert_element_type.94, f32[]{:T(128)S(6)} %convert_element_type.93, ...), kind=kOutput, calls=%fused_computation.3 | convolution fusion | flops 35913728 | bytes 4458560 | tf_op jit(solution)/shard_map/dot_general | solution.py:505
  10.3 0.0 copy-start.2
  10.3 3.5 %all-to-all-start = ((bf16[4,64,256]{2,1,0:T(8,128)(2,1)}), bf16[4,64,256]{2,1,0:T(8,128)(2,1)S(1)}, u32[]{:S(2)}, u32[]{:S(2)}) async-start(bf16[4,64,256]{2,1,0:T(8,128)(2,1)} %bitcast.1), calls=%async_computation | async-start | bytes 262144 | tf_op jit(solution)/shard_map/all_to_all | solution.py:508
  13.8 4.5 %all-to-all-done = bf16[4,64,256]{2,1,0:T(8,128)(2,1)S(1)} async-done(((bf16[4,64,256]{2,1,0:T(8,128)(2,1)}), bf16[4,64,256]{2,1,0:T(8,128)(2,1)S(1)}, u32[]{:S(2)}, u32[]{:S(2)}) %all-to-all-start) | async-done | bytes 131104 | tf_op jit(solution)/shard_map/all_to_all | solution.py:508
  18.4 3.2 %fusion.2 = (f32[64]{0:T(128)S(1)}, bf16[64,2048]{1,0:T(8,128)(2,1)S(1)}) fusion(bf16[64,1024]{1,0:T(8,128)(2,1)S(1)} %bitcast.10, bf16[1024,2048]{1,0:T(8,128)(2,1)} %param.18, bf16[256,2048]{1,0:T(8,128)(2,1)} %param.14, s32[]{:T(128)S(6)} %select_n.9), kind=kOutput, calls=%fused_computation.6 | convolution fusion | flops 269221824 | bytes 4849924 | tf_op jit(solution)/shard_map/dot_general | solution.py:509
  21.6 0.0 copy-start.1
  21.6 0.0 copy-done.2
  21.6 0.1 fusion.4
  21.8 0.8 concatenate.10.packed_ref
  22.5 0.0 copy-done.1
  22.5 110.0 %exchange_experts.1 = bf16[64,2048]{1,0:T(8,128)(2,1)} custom-call(bf16[64,2176]{1,0:T(8,128)(2,1)} %concatenate.10.packed_ref, bf16[64,2048]{1,0:T(8,128)(2,1)} %copy-done.1, bf16[1,2048,512]{2,1,0:T(8,128)(2,1)} %gate_hbm.1, bf16[1,2048,512]{2,1,0:T(8,128)(2,1)} %up_hbm.1, bf16[1,512,2048]{2,1,0:T(8,128)(2,1)} %down_hbm.1, bf16[2048,128]{1,0:T(8,128)(2,1)} %sgate_hbm.1, ...), custom_call_target="tpu_custom_call" | custom-call | tf_op jit(solution)/shard_map/exchange_experts/pallas_call | solution.py:436
  132.6 1.7 %copy.26 = bf16[64,2048]{1,0:T(8,128)(2,1)} copy(bf16[64,2048]{1,0:T(8,128)(2,1)} %exchange_experts.1) | data formatting | bytes 524288
  (4 shorter events, 0.0 us)
Async XLA Ops:
  0.0 8.3 %copy-start = (bf16[1,256,256]{2,1,0:T(8,128)(2,1)S(1)}, bf16[1,256,256]{2,1,0:T(8,128)(2,1)}, u32[]{:S(2)}) copy-start(bf16[1,256,256]{2,1,0:T(8,128)(2,1)} %param.16) | copy-start | bytes 393220
  0.7 6.6 %collective-permute-start = (bf16[15,256]{1,0:T(8,128)(2,1)S(1)}, bf16[15,256]{1,0:T(8,128)(2,1)S(1)}, u32[]{:S(2)}, u32[]{:S(2)}) collective-permute-start(bf16[15,256]{1,0:T(8,128)(2,1)S(1)} %slice.52), channel_id=1, source_target_pairs={{0,4},{4,8},{8,12},{12,16},{16,20},{20,24},{24,28},{1,5},{5,9},{9,... | collective-permute-start | bytes 23048 | tf_op jit(solution)/shard_map/ppermute | solution.py:19
  10.3 11.3 %copy-start.2 = (f32[2048]{0:T(1024)S(1)}, f32[2048]{0:T(1024)}, u32[]{:S(2)}) copy-start(f32[2048]{0:T(1024)} %param.19) | copy-start | bytes 24580
  10.3 8.0 %all-to-all-start = ((bf16[4,64,256]{2,1,0:T(8,128)(2,1)}), bf16[4,64,256]{2,1,0:T(8,128)(2,1)S(1)}, u32[]{:S(2)}, u32[]{:S(2)}) async-start(bf16[4,64,256]{2,1,0:T(8,128)(2,1)} %bitcast.1), calls=%async_computation | async-start | bytes 262144 | tf_op jit(solution)/shard_map/all_to_all | solution.py:508
  21.6 1.0 copy-start.1

commit v2 on v1

--- a/solution.py
+++ b/solution.py
@@ -139,8 +139,14 @@
     nz,
     rows,
     width,
-    packed_ref,
-    resid_ref,
+    pooled_ref,
+    pmap_ref,
+    pscale_ref,
+    gain_ref,
+    routes_ref,
+    rweights_ref,
+    stream_hbm,
+    owt_hbm,
     gate_hbm,
     up_hbm,
     down_hbm,
@@ -166,8 +172,16 @@
     wsgate,
     wsup,
     wsdown,
+    wout,
+    resid,
+    rim,
+    gmix,
+    mixbuf,
     wsem,
-    osem,
+    rim_s,
+    rim_r,
+    mix_s,
+    mix_r,
     zs,
     zr,
     a_s,
@@ -213,7 +227,12 @@
     def blk(cls, d, j):
         return gbuf.at[cls, d, pl.ds(j * rows, rows)]
 
+    tok_dev = pooled_ref.shape[0]
+    sp_size, tp_size = nz * 2, mixbuf.shape[0]
+    own_rows = pl.ds(pl.multiple_of(tp * rows, rows), rows)
     weight_pairs = (
+        (owt_hbm, wout),
+        (stream_hbm.at[own_rows], resid),
         (gate_hbm.at[0], wgate),
         (up_hbm.at[0], wup),
         (down_hbm.at[0], wdown),
@@ -224,25 +243,78 @@
     weight_copies = [
         pltpu.make_async_copy(s, t, wsem.at[i]) for i, (s, t) in enumerate(weight_pairs)
     ]
-    own_copy = pltpu.make_async_copy(packed_ref, blk(0, 0, 0), osem)
-    own_copy.start()
     for copy in weight_copies:
         copy.start()
 
+    ahead = (sp + 1) % sp_size
+
+    def rim_copy():
+        last = pl.ds(tok_dev - REACH, REACH)
+        return rdma(pooled_ref.at[last], rim, rim_s, rim_r, (ahead, tp))
+
+    def mix_copy(k):
+        there = (tp + k) % tp_size
+        part = pl.ds(pl.multiple_of(there * rows, rows), rows)
+        return rdma(gmix.at[part], mixbuf.at[tp], mix_s.at[k], mix_r.at[tp], (sp, there))
+
+    def mix_recv(k):
+        here = (tp + k) % tp_size
+        return rdma(gmix.at[pl.ds(0, rows)], mixbuf.at[here], mix_s.at[k], mix_r.at[here], (sp, here))
+
     barrier = pltpu.get_barrier_semaphore()
-    peers = [peer_z(k) for k in range(1, nz)] + [peer_a, peer_b, peer_c]
+
+    def greet(peer):
+        pl.semaphore_signal(barrier, inc=1, device_id=peer, device_id_type=pl.DeviceIdType.MESH)
+
+    peers = [peer_z(k) for k in range(1, nz)] + [dev(z, 1 - y, x, c)]
+    peers = peers + [(sp, (tp + k) % tp_size) for k in range(1, tp_size)]
+    slant = sp + 2 * y - 1
+    slanted = (slant >= 0) & (slant < sp_size)
     for peer in peers:
-        pl.semaphore_signal(
-            barrier, inc=1, device_id=peer, device_id_type=pl.DeviceIdType.MESH
+        greet(peer)
+    pl.when(slanted)(lambda: greet(((slant + sp_size) % sp_size, tp)))
+    pl.semaphore_wait(barrier, len(peers) + jnp.where(slanted, 1, 0))
+
+    near_first = [
+        sorted(range(nz), key=lambda k: (abs(k - at), k if 2 * at < nz else -k))
+        for at in range(nz)
+    ]
+
+    def source_at(at, slot):
+        found = jnp.int32(0)
+        for i in range(nz):
+            for j in range(nz):
+                found = jnp.where((at == i) & (slot == j), near_first[i][j], found)
+        return found
+
+    def slot_at(at, source):
+        found = jnp.int32(0)
+        for i in range(nz):
+            for j in range(nz):
+                found = jnp.where((at == i) & (source == j), near_first[i].index(j), found)
+        return found
+
+    def z_copy(slot, source, step):
+        there = (z + step + nz) % nz
+        landing = slot_at(there, source)
+        index = 2 * slot + (1 if step > 0 else 0)
+        return rdma(
+            blk(0, slot, 0), blk(0, landing, 0), zs.at[index], zr.at[landing], dev(there, y, x, c)
         )
-    pl.semaphore_wait(barrier, len(peers))
-    own_copy.wait()
-
-    def z_copy(k):
-        return rdma(blk(0, 0, 0), blk(0, nz - k, 0), zs.at[k], zr.at[nz - k], peer_z(k))
+
+    def z_each(slot, act):
+        source = z if isinstance(slot, int) and slot == 0 else source_at(z, slot)
+
+        @pl.when((source <= z) & (z < nz - 1))
+        def _():
+            act(z_copy(slot, source, 1))
+
+        @pl.when((source >= z) & (z > 0))
+        def _():
+            act(z_copy(slot, source, -1))
 
     def z_recv(d):
-        return rdma(blk(0, 0, 0), blk(0, d, 0), zs.at[d], zr.at[d], peer_z(d))
+        return rdma(blk(0, 0, 0), blk(0, d, 0), zs.at[d], zr.at[d], peer_z(1))
 
     def a_copy(d):
         return rdma(blk(0, d, 0), blk(0, d, 1), a_s.at[d], a_r.at[d], peer_a)
@@ -252,6 +324,67 @@
 
     def c_copy(d, j):
         return rdma(blk(0, d, j), blk(1, d, j), cs.at[4 * d + j], cr.at[4 * d + j], peer_c)
+
+    def mixer():
+        @pl.when(sp < sp_size - 1)
+        def _():
+            rim_copy().start()
+
+        named = routes_ref[own_rows, :]
+        given = rweights_ref[own_rows, :]
+        lane = lax.broadcasted_iota(jnp.int32, (rows, LANES), 1)
+        table = jnp.zeros((rows, LANES), jnp.float32)
+        for k in range(named.shape[1]):
+            hit = lane % (LANES // 2) == named[:, k : k + 1]
+            table = table + jnp.where(hit, given[:, k : k + 1], 0.0)
+        high = table.astype(jnp.bfloat16).astype(jnp.float32)
+        tags = jnp.where(lane < LANES // 2, high, table - high).astype(jnp.bfloat16)
+        gbuf[0, 0, 0:rows, width : width + LANES] = tags
+
+        @pl.when(sp == 0)
+        def _():
+            rim[...] = jnp.zeros_like(rim)
+
+        @pl.when(sp > 0)
+        def _():
+            rim_copy().wait_recv()
+
+        own = pooled_ref[...].astype(jnp.float32)
+        summed = jnp.concatenate([rim[...].astype(jnp.float32), own], 0)
+        window = 2
+        chosen = jnp.zeros_like(summed)
+        for group in range(tp_size):
+            summed = summed + pltpu.roll(summed, window // 2, 0)
+            chosen = jnp.where(tp == group, summed, chosen)
+            window = 2 * window
+        mine = lax.shift_left(jnp.int32(2), tp)
+        position = sp * tok_dev + lax.broadcasted_iota(jnp.int32, (tok_dev, 1), 0)
+        counted = jnp.minimum(position + 1, mine).astype(jnp.float32)
+        pooled = (chosen[REACH:] / counted - own).astype(jnp.bfloat16)
+        mapped = jnp.dot(pooled, pmap_ref[0], preferred_element_type=jnp.float32)
+        gmix[...] = (mapped * pscale_ref[...]).astype(jnp.bfloat16)
+        for k in range(1, tp_size):
+            mix_copy(k).start()
+        mixbuf[tp] = gmix[own_rows, :]
+        weight_copies[0].wait()
+        weight_copies[1].wait()
+        for k in range(1, tp_size):
+            mix_recv(k).wait_recv()
+        grouped = jnp.concatenate([mixbuf[k] for k in range(tp_size)], 1)
+        squares = jnp.zeros((rows, 1), jnp.float32)
+        step = min(512, width)
+        for i in range(width // step):
+            cols = slice(i * step, (i + 1) * step)
+            mixed = jnp.dot(grouped, wout[:, cols], preferred_element_type=jnp.float32)
+            after = (resid[:, cols].astype(jnp.float32) + mixed).astype(jnp.bfloat16)
+            resid[:, cols] = after
+            after = after.astype(jnp.float32)
+            squares = squares + jnp.sum(after * after, axis=1, keepdims=True)
+        factor = lax.rsqrt(squares / width + EPSILON)
+        for i in range(width // step):
+            cols = slice(i * step, (i + 1) * step)
+            normed = resid[:, cols].astype(jnp.float32) * factor * gain_ref[:, cols]
+            gbuf[0, 0, 0:rows, cols] = normed.astype(jnp.bfloat16)
 
     def first_pass(d):
         a_copy(d).start()
@@ -266,17 +399,23 @@
     def rc_copy(d):
         return rdma(pbuf.at[d], rcbuf.at[d], rcs.at[d], rcr.at[d], peer_c)
 
-    def rb_copy(d):
-        return rdma(sbuf_b.at[d], rbuf_b.at[d], rbs.at[d], rbr.at[d], peer_b)
+    def rb_copy(d, a):
+        part = pl.ds(a * rows, rows)
+        sems = rbs.at[2 * d + a], rbr.at[2 * d + a]
+        return rdma(sbuf_b.at[d, part], rbuf_b.at[d, part], *sems, peer_b)
 
     def ra_copy(d):
         return rdma(sbuf_a.at[d], rbuf_a.at[d], ras.at[d], rar.at[d], peer_a)
 
     def rz_copy(d):
-        return rdma(sbuf_z.at[d], rbuf_z.at[nz - d], rzs.at[d], rzr.at[nz - d], peer_z(d))
+        there = source_at(z, d)
+        landing = slot_at(there, z)
+        return rdma(
+            sbuf_z.at[d], rbuf_z.at[landing], rzs.at[d], rzr.at[landing], dev(there, y, x, c)
+        )
 
     def rz_recv(d):
-        return rdma(sbuf_z.at[d], rbuf_z.at[d], rzs.at[d], rzr.at[d], peer_z(d))
+        return rdma(sbuf_z.at[d], rbuf_z.at[d], rzs.at[d], rzr.at[d], peer_z(1))
 
     dot = functools.partial(jnp.dot, preferred_element_type=jnp.float32)
     step_in = min(256, wgate.shape[1])
@@ -326,12 +465,15 @@
 
     def reduce_b(d):
         rc_copy(d).wait_recv()
-        upper = pl.ds(2 * rows, 2 * rows)
-        sbuf_b[d] = (acc[d, upper, :] + wide(rcbuf[d, upper, :])).astype(jnp.bfloat16)
-        rb_copy(d).start()
+        for a in (1, 0):
+            here = pl.ds(a * rows, rows)
+            part = pl.ds((2 + a) * rows, rows)
+            total = acc[d, part, :] + wide(rcbuf[d, part, :])
+            sbuf_b[d, here, :] = total.astype(jnp.bfloat16)
+            rb_copy(d, a).start()
 
     def reduce_a(d):
-        rb_copy(d).wait_recv()
+        rb_copy(d, 1).wait_recv()
         part = pl.ds(rows, rows)
         total = acc[d, part, :] + wide(rcbuf[d, part, :]) + wide(rbuf_b[d, part, :])
         sbuf_a[d] = total.astype(jnp.bfloat16)
@@ -347,49 +489,64 @@
         )
 
     def reduce_z(d):
+        rb_copy(d, 0).wait_recv()
         ra_copy(d).wait_recv()
 
         @pl.when(d > 0)
         def _():
-            sbuf_z[d] = base_total(d).astype(jnp.bfloat16)
-            rz_copy(d).start()
-
-    for k in range(1, nz):
-        z_copy(k).start()
-    first_pass(0)
-    second_pass(0)
-    for copy in weight_copies:
-        copy.wait()
-
-    @pl.loop(0, nz)
-    def _(d):
-        @pl.when(d < nz - 1)
-        def _():
-            z_recv(d + 1).wait_recv()
-            first_pass(d + 1)
-
+            send_z(d)
+
+    def send_z(d):
+        sbuf_z[d] = base_total(d).astype(jnp.bfloat16)
+        rz_copy(d).start()
+
+    def z_arrival(d):
+        z_recv(d).wait_recv()
+        z_each(d, lambda copy: copy.start())
+        first_pass(d)
+
+    def b_arrival(d):
         for a in range(2):
             b_copy(d, a).wait_recv()
             c_copy(d, 2 + a).start()
 
+    mixer()
+    z_each(0, lambda copy: copy.start())
+    first_pass(0)
+    z_arrival(1)
+    second_pass(0)
+    b_arrival(0)
+    for copy in weight_copies[2:]:
+        copy.wait()
+
+    @pl.loop(0, nz)
+    def _(d):
+        @pl.when(d + 2 < nz)
+        def _():
+            z_arrival(d + 2)
+
+        @pl.when(d + 1 < nz)
+        def _():
+            second_pass(d + 1)
+
+        for j in range(4):
+            c_copy(d, j).wait_recv()
+
+        def store_part(cols, value):
+            pbuf[d, :, cols] = value.astype(jnp.bfloat16)
+
+        expert(1, d, store_part)
+        rc_copy(d).start()
+
         def store_acc(cols, value):
             acc[d, :, cols] = value
 
         expert(0, d, store_acc)
-
-        @pl.when(d < nz - 1)
-        def _():
-            second_pass(d + 1)
-
-        for j in range(4):
-            c_copy(d, j).wait_recv()
-
-        def store_part(cols, value):
-            pbuf[d, :, cols] = value.astype(jnp.bfloat16)
-
-        expert(1, d, store_part)
-        rc_copy(d).start()
         reduce_b(d)
+
+        @pl.when(d + 1 < nz)
+        def _():
+            b_arrival(d + 1)
 
         @pl.when(d >= 1)
         def _():
@@ -402,31 +559,39 @@
     reduce_a(nz - 1)
     reduce_z(nz - 2)
     reduce_z(nz - 1)
-    total = base_total(0) + wide(resid_ref[...])
+    total = base_total(0) + wide(resid[...])
     for d in range(1, nz):
         rz_recv(d).wait_recv()
         total = total + wide(rbuf_z[d])
     out_ref[...] = total.astype(jnp.bfloat16)
 
+    pl.when(sp < sp_size - 1)(lambda: rim_copy().wait_send())
+    for k in range(1, tp_size):
+        mix_copy(k).wait_send()
     for k in range(1, nz):
-        z_copy(k).wait_send()
         rz_copy(k).wait_send()
+
+    z_each(0, lambda copy: copy.wait_send())
+    for k in range(1, nz):
+        z_each(k, lambda copy: copy.wait_send())
 
     @pl.loop(0, nz)
     def _(d):
         a_copy(d).wait_send()
         for a in range(2):
             b_copy(d, a).wait_send()
+            rb_copy(d, a).wait_send()
         for j in range(4):
             c_copy(d, j).wait_send()
         rc_copy(d).wait_send()
-        rb_copy(d).wait_send()
         ra_copy(d).wait_send()
 
 
-def exchanged(packed, resid, weights, nz):
-    rows, width = resid.shape
-    gate, up, down, sgate, sup, sdown = weights
+def exchanged(small, large, rows, nz):
+    pooled_in = small[0]
+    stream, out_weight, gate, up, down, sgate, sup, sdown = large
+    width = stream.shape[1]
+    tok_dev, group_width = pooled_in.shape
     bf16, f32 = jnp.bfloat16, jnp.float32
     four, two = 4 * rows, 2 * rows
     vm = pltpu.VMEM
@@ -436,7 +601,7 @@
     return pl.pallas_call(
         functools.partial(exchange_kernel, nz, rows, width),
         out_shape=jax.ShapeDtypeStruct((rows, width), bf16),
-        in_specs=[vmem_spec] * 2 + [any_spec] * 6,
+        in_specs=[vmem_spec] * len(small) + [any_spec] * len(large),
         out_specs=vmem_spec,
         scratch_shapes=[
             vm((2, nz, four, width + LANES), bf16),
@@ -457,16 +622,24 @@
             vm(sgate.shape, bf16),
             vm(sup.shape, bf16),
             vm(sdown.shape, bf16),
-            dma((6,)),
+            vm(out_weight.shape, bf16),
+            vm((rows, width), bf16),
+            vm((REACH, group_width), bf16),
+            vm((tok_dev, group_width), bf16),
+            vm((tok_dev // rows, rows, group_width), bf16),
+            dma((len(large),)),
             dma,
+            dma,
+            dma((tok_dev // rows,)),
+            dma((tok_dev // rows,)),
         ]
-        + [dma((n,)) for n in (nz, nz, nz, nz, 2 * nz, 2 * nz, 4 * nz, 4 * nz)]
-        + [dma((nz,)) for _ in range(8)],
+        + [dma((n,)) for n in (2 * nz, nz, nz, nz, 2 * nz, 2 * nz, 4 * nz, 4 * nz)]
+        + [dma((n,)) for n in (nz, nz, 2 * nz, 2 * nz, nz, nz, nz, nz)],
         compiler_params=pltpu.CompilerParams(
             collective_id=0, has_side_effects=True, vmem_limit_bytes=60 * 2**20
         ),
         name="exchange_experts",
-    )(packed, resid, gate, up, down, sgate, sup, sdown)
+    )(*small, *large)
 
 
 def on_device_dense(
@@ -485,47 +658,11 @@
     shared_up,
     shared_down,
 ):
-    tok_dev, group_width = pooled_in.shape
-    tp_size = lax.axis_size("tp")
-    sp_size = lax.axis_size("sp")
-    tp_index = lax.axis_index("tp")
-    sp_index = lax.axis_index("sp")
-    rows_dev = tok_dev // tp_size
-    window = lax.shift_left(jnp.int32(2), tp_index)
-    rim_rows = passed_along(pooled_in[tok_dev - (REACH - 1) :], "sp", 1)
-    padded = jnp.concatenate([rim_rows, pooled_in], 0).astype(jnp.float32)
-    summed = jnp.zeros((tok_dev, group_width), jnp.float32)
-    for lag_step in range(REACH):
-        enabled = (lag_step < window).astype(jnp.float32)
-        summed = summed + padded[REACH - 1 - lag_step : REACH - 1 - lag_step + tok_dev] * enabled
-    position = sp_index * tok_dev + jnp.arange(tok_dev, dtype=jnp.int32)
-    counted = jnp.minimum(position + 1, window).astype(jnp.float32)
-    pooled = (summed / counted[:, None] - padded[REACH - 1 :]).astype(jnp.bfloat16)
-    group_mix = (
-        jnp.dot(pooled, pool_weight[0], preferred_element_type=jnp.float32) * pool_scale
-    ).astype(jnp.bfloat16)
-    own_begin = tp_index * rows_dev
-    own_mix = lax.all_to_all(group_mix, "tp", split_axis=0, concat_axis=1, tiled=True)
-    mixed_all = jnp.dot(own_mix, out_weight, preferred_element_type=jnp.float32)
-    own_stream = lax.dynamic_slice_in_dim(stream, own_begin, rows_dev, 0)
-    residual = (own_stream.astype(jnp.float32) + mixed_all).astype(jnp.bfloat16)
-    resid_wide = residual.astype(jnp.float32)
-    normed = (
-        resid_wide
-        * lax.rsqrt(jnp.mean(resid_wide * resid_wide, axis=-1, keepdims=True) + EPSILON)
-        * norm_gain
-    ).astype(jnp.bfloat16)
-    own_routes = lax.dynamic_slice_in_dim(routes, own_begin, rows_dev, 0)
-    own_weights = lax.dynamic_slice_in_dim(route_weights, own_begin, rows_dev, 0)
-    ids = jnp.arange(LANES // 2, dtype=jnp.int32)
-    table = jnp.sum(
-        jnp.where(own_routes[:, :, None] == ids, own_weights[:, :, None], 0.0), axis=1
-    )
-    high = lax.reduce_precision(table, 8, 7)
-    tags = jnp.concatenate([high, table - high], 1).astype(jnp.bfloat16)
-    packed = jnp.concatenate([normed, tags], 1)
-    weights = (expert_gate, expert_up, expert_down, shared_gate, shared_up, shared_down)
-    return exchanged(packed, residual, weights, sp_size // 2)
+    nz = lax.axis_size("sp") // 2
+    rows_dev = pooled_in.shape[0] // lax.axis_size("tp")
+    small = (pooled_in, pool_weight, pool_scale[None], norm_gain[None], routes, route_weights)
+    large = (stream, out_weight, expert_gate, expert_up, expert_down)
+    return exchanged(small, large + (shared_gate, shared_up, shared_down), rows_dev, nz)
 
 
 def held_whole(mesh, *args):

time: 135 us -> 116 us (0.86)
  starting transfers between devices: 8.34 us -> 0 us
  matrix products: 5.21 us -> 0 us
  waiting for transfers between devices: 4.55 us -> 0 us
    dot_general x2 -> x0, matrix products: 5.21 us -> none  [the longest x1 3.18 us: on_device_dense(): mixed_all = jnp.dot(own_mix, out_weight, preferred_element_type=jnp.float32)]
    ppermute x1 -> x0, starting transfers between devices: 4.89 us -> none  [passed_along(): lax.ppermute(value, axis, [(source, source + steps) for source in range(i...]
    all_to_all x1 -> x0, waiting for transfers between devices: 4.55 us -> none  [on_device_dense(): lax.all_to_all(group_mix, 'tp', split_axis=0, concat_axis=1, tiled=True)]
    all_to_all x1 -> x0, starting transfers between devices: 3.46 us -> none  [on_device_dense(): lax.all_to_all(group_mix, 'tp', split_axis=0, concat_axis=1, tiled=True)]
    unnamed x7 -> x3, local copies, waits for them, and re-layouts: 1.68 us -> 4.63 us
    dynamic_slice x2 -> x0, local copies, waits for them, and re-layouts: 1.51 us -> none  [the longest x1 0.76 us: on_device_dense(): own_routes = lax.dynamic_slice_in_dim(routes, own_begin, rows_dev, 0)]
  transfers between devices with their start and end apart: 2 -> 0, of which waited for: 1 -> 0; matrix products, arithmetic and copies ran while one was open for 1% -> 0% of each run, Pallas kernels for 0% -> 0%
where the time goes in v2:
time: 116 us; the launch traced here: 115 us
  Pallas kernels  111 us (96%)
  local copies, waits for them, and re-layouts  4.63 us (4%)
    pallas_call x1, Pallas kernels, exchanged(): pl.pallas_call(functools.partial(exchange_kernel, nz, rows, width), out_s...  111 us
    unnamed x3, local copies, waits for them, and re-layouts  4.63 us

profile of v2, /device:TPU:0, one launch (start us, length us, event | category | flops | bytes accessed | tf_op | source)
XLA Modules:
  0.0 115.3 jit_solution(21072393032772884)
XLA Ops:
  0.0 1.5 %copy.15.routes_ref = s32[256,3]{1,0:T(8,128)} copy(s32[256,3]{0,1:T(4,128)} %param.20) | data formatting | bytes 6144 | tf_op args[6]
  1.5 1.5 %copy.16.rweights_ref = f32[256,3]{1,0:T(8,128)} copy(f32[256,3]{0,1:T(4,128)} %param.21) | data formatting | bytes 6144 | tf_op args[7]
  3.0 110.7 %exchange_experts.1 = bf16[64,2048]{1,0:T(8,128)(2,1)} custom-call(bf16[256,256]{1,0:T(8,128)(2,1)} %pooled_ref.1, bf16[1,256,256]{2,1,0:T(8,128)(2,1)} %pmap_ref.1, f32[1,256]{1,0:T(1,128)} %bitcast.3, f32[1,2048]{1,0:T(1,128)} %bitcast.2, s32[256,3]{1,0:T(8,128)} %copy.15.routes_ref, f32[256,3]{1,0:T(8,128)} %copy.16.rweights_ref, ...), custom_call_target="tpu_custom_call" | custom-call | tf_op jit(solution)/shard_map/exchange_experts/pallas_call | solution.py:601
  113.7 1.7 %copy.18 = bf16[64,2048]{1,0:T(8,128)(2,1)} copy(bf16[64,2048]{1,0:T(8,128)(2,1)} %exchange_experts.1) | data formatting | bytes 524288

commit v3 on v2

--- a/solution.py
+++ b/solution.py
@@ -275,8 +275,8 @@
     pl.when(slanted)(lambda: greet(((slant + sp_size) % sp_size, tp)))
     pl.semaphore_wait(barrier, len(peers) + jnp.where(slanted, 1, 0))
 
-    near_first = [
-        sorted(range(nz), key=lambda k: (abs(k - at), k if 2 * at < nz else -k))
+    far_first = [
+        sorted(range(nz), key=lambda k: (k != at, -abs(k - at), k))
         for at in range(nz)
     ]
 
@@ -284,34 +284,22 @@
         found = jnp.int32(0)
         for i in range(nz):
             for j in range(nz):
-                found = jnp.where((at == i) & (slot == j), near_first[i][j], found)
+                found = jnp.where((at == i) & (slot == j), far_first[i][j], found)
         return found
 
     def slot_at(at, source):
         found = jnp.int32(0)
         for i in range(nz):
             for j in range(nz):
-                found = jnp.where((at == i) & (source == j), near_first[i].index(j), found)
+                found = jnp.where((at == i) & (source == j), far_first[i].index(j), found)
         return found
 
-    def z_copy(slot, source, step):
-        there = (z + step + nz) % nz
-        landing = slot_at(there, source)
-        index = 2 * slot + (1 if step > 0 else 0)
+    def z_copy(d):
+        there = source_at(z, d)
+        landing = slot_at(there, z)
         return rdma(
-            blk(0, slot, 0), blk(0, landing, 0), zs.at[index], zr.at[landing], dev(there, y, x, c)
+            blk(0, 0, 0), blk(0, landing, 0), zs.at[d], zr.at[landing], dev(there, y, x, c)
         )
-
-    def z_each(slot, act):
-        source = z if isinstance(slot, int) and slot == 0 else source_at(z, slot)
-
-        @pl.when((source <= z) & (z < nz - 1))
-        def _():
-            act(z_copy(slot, source, 1))
-
-        @pl.when((source >= z) & (z > 0))
-        def _():
-            act(z_copy(slot, source, -1))
 
     def z_recv(d):
         return rdma(blk(0, 0, 0), blk(0, d, 0), zs.at[d], zr.at[d], peer_z(1))
@@ -502,7 +490,6 @@
 
     def z_arrival(d):
         z_recv(d).wait_recv()
-        z_each(d, lambda copy: copy.start())
         first_pass(d)
 
     def b_arrival(d):
@@ -511,7 +498,8 @@
             c_copy(d, 2 + a).start()
 
     mixer()
-    z_each(0, lambda copy: copy.start())
+    for k in range(1, nz):
+        z_copy(k).start()
     first_pass(0)
     z_arrival(1)
     second_pass(0)
@@ -571,9 +559,8 @@
     for k in range(1, nz):
         rz_copy(k).wait_send()
 
-    z_each(0, lambda copy: copy.wait_send())
     for k in range(1, nz):
-        z_each(k, lambda copy: copy.wait_send())
+        z_copy(k).wait_send()
 
     @pl.loop(0, nz)
     def _(d):
@@ -633,7 +620,7 @@
             dma((tok_dev // rows,)),
             dma((tok_dev // rows,)),
         ]
-        + [dma((n,)) for n in (2 * nz, nz, nz, nz, 2 * nz, 2 * nz, 4 * nz, 4 * nz)]
+        + [dma((n,)) for n in (nz, nz, nz, nz, 2 * nz, 2 * nz, 4 * nz, 4 * nz)]
         + [dma((n,)) for n in (nz, nz, 2 * nz, 2 * nz, nz, nz, nz, nz)],
         compiler_params=pltpu.CompilerParams(
             collective_id=0, has_side_effects=True, vmem_limit_bytes=60 * 2**20

time: 116 us -> 109 us (0.940)
  Pallas kernels: 111 us -> 104 us
    pallas_call x1, Pallas kernels: 111 us -> 104 us  [exchanged(): pl.pallas_call(functools.partial(exchange_kernel, nz, rows, width), out_s...]
where the time goes in v3:
time: 109 us
  Pallas kernels  104 us (95%)
  local copies, waits for them, and re-layouts  4.63 us (4%)
    pallas_call x1, Pallas kernels, exchanged(): pl.pallas_call(functools.partial(exchange_kernel, nz, rows, width), out_s...  104 us
    unnamed x3, local copies, waits for them, and re-layouts  4.63 us

profile of v3, /device:TPU:0, one launch (start us, length us, event | category | flops | bytes accessed | tf_op | source)
XLA Modules:
  0.0 108.6 jit_solution(3610890618286852020)
XLA Ops:
  0.0 1.5 %copy.15.routes_ref = s32[256,3]{1,0:T(8,128)} copy(s32[256,3]{0,1:T(4,128)} %param.20) | data formatting | bytes 6144 | tf_op args[6]
  1.5 1.5 %copy.16.rweights_ref = f32[256,3]{1,0:T(8,128)} copy(f32[256,3]{0,1:T(4,128)} %param.21) | data formatting | bytes 6144 | tf_op args[7]
  3.0 103.9 %exchange_experts.1 = bf16[64,2048]{1,0:T(8,128)(2,1)} custom-call(bf16[256,256]{1,0:T(8,128)(2,1)} %pooled_ref.1, bf16[1,256,256]{2,1,0:T(8,128)(2,1)} %pmap_ref.1, f32[1,256]{1,0:T(1,128)} %bitcast.3, f32[1,2048]{1,0:T(1,128)} %bitcast.2, s32[256,3]{1,0:T(8,128)} %copy.15.routes_ref, f32[256,3]{1,0:T(8,128)} %copy.16.rweights_ref, ...), custom_call_target="tpu_custom_call" | custom-call | tf_op jit(solution)/shard_map/exchange_experts/pallas_call | solution.py:588
  106.9 1.7 %copy.18 = bf16[64,2048]{1,0:T(8,128)(2,1)} copy(bf16[64,2048]{1,0:T(8,128)(2,1)} %exchange_experts.1) | data formatting | bytes 524288
